TPU v7x, 32 devices: a whole 2x2x4 slice. The times are simulated.
32 devices in a mesh: grp: 2 (over y), fs: 4 (over z), tp: 4 (over x, core).
Axes of the slice: x: 2, y: 2, z: 4, core: 2. Of those that a mesh axis runs over, the one named last changes fastest.
Arguments:
- tokens: bfloat16 [6144, 2048], P(('grp', 'fs'), 'tp'), parts along dimension 0, may hold values from -6 to 6
- mix_gain: float32 [2048], replicated, may hold values from 0.1 to 1.9
- w_u: float32 [2048, 1024], P('fs', 'tp'), may hold values from -0.125 to 0.125
- w_v: float32 [2048, 1024], P('fs', 'tp'), may hold values from -0.125 to 0.125
- u_scale: float32 [1024], P('tp'), may hold values from 0.5 to 2
- v_scale: float32 [1024], P('tp'), may hold values from 0.5 to 2
- spatial: bfloat16 [8, 128, 128], P('tp'), may hold values from -0.5 to 0.5
- spatial_bias: float32 [8, 128], P('tp'), may hold values from 0.1 to 1.9
- w_mix: float32 [1024, 2048], P('tp', 'fs'), may hold values from -0.1875 to 0.1875
- mix_scale: float32 [1, 2048], P(None, 'fs'), may hold values from 0.5 to 2
- ffn_gain: float32 [2048], replicated, may hold values from 0.1 to 1.9
- w_gate: float32 [2048, 5632], P('fs', 'tp'), may hold values from -0.125 to 0.125
- w_up: float32 [2048, 5632], P('fs', 'tp'), may hold values from -0.125 to 0.125
- gate_scale: float32 [5632], P('tp'), may hold values from 0.5 to 2
- up_scale: float32 [5632], P('tp'), may hold values from 0.5 to 2
- w_down: float32 [5632, 2048], P('tp', 'fs'), may hold values from -0.078125 to 0.078125
- down_scale: float32 [1, 2048], P(None, 'fs'), may hold values from 0.5 to 2
Outputs:
- layer_out: bfloat16 [6144, 2048], P(('grp', 'fs'), 'tp'), parts along dimension 0
There are 2 independent parts, one for each index of `grp`. A program takes and returns all parts, laid end to end along the dimension named above; an argument that names none is the same for every part. Nothing has to cross between parts.
All inputs are finite; a program needn't handle non-finite values.
Results may differ from a plain program's by a relative error of at most 0.024.
Values may be sent and summed in bfloat16 or wider, within the bound.
A program may use at most 128 MiB of HBM per device.

v0:
```python
import functools

import jax
import jax.numpy as jnp
from jax import lax
from jax.experimental import pallas as pl
from jax.experimental.pallas import tpu as pltpu
from jax.sharding import PartitionSpec as P

MESH = pl.DeviceIdType.MESH
eps = 1e-06
H = 2
half_root = 0.7071067811865476


def gelu(a):
    return 0.5 * a * (1.0 + lax.erf(a * half_root))


def layer_kernel(
    dims,
    tokens,
    gains,
    w_uv,
    w_mix,
    w_gate,
    w_up,
    w_down,
    uv_scale,
    spatial,
    bias,
    scales,
    ffn_scale,
    out,
    uv_buf,
    mix_buf,
    gate_buf,
    up_buf,
    down_buf,
    scale_buf,
    tok_buf,
    res_buf,
    normed,
    gated,
    silu_buf,
    act,
    resid,
    give_buf,
    send_buf,
    pair_buf,
    far_buf,
    keep,
    z_send,
    z_recv,
    y_send,
    y_recv,
    w_local,
    s_send,
    s_recv,
    s_local,
    g_send,
    g_fwd,
    g_recv,
    g_local,
    p_send,
    p_recv,
    f_send,
    f_recv,
):
    n, n_tp = dims
    nx = n_tp // 2
    i = lax.axis_index("fs")
    g = lax.axis_index("grp")
    t = lax.axis_index("tp")
    x, c = t // 2, t % 2
    rows, dt = tokens.shape
    df = scales.shape[1]
    per = dt // df
    rt = rows // H
    partner = {"tp": x * 2 + 1 - c}
    across = {"grp": 1 - g}

    def remote(src, dst, ss, rs, device):
        return pltpu.make_async_remote_copy(
            src_ref=src,
            dst_ref=dst,
            send_sem=ss,
            recv_sem=rs,
            device_id=device,
            device_id_type=MESH,
        )

    barrier = pltpu.get_barrier_semaphore()
    for k in range(1, n):
        pl.semaphore_signal(barrier, 1, device_id={"fs": (i + k) % n}, device_id_type=MESH)
    pl.semaphore_signal(barrier, 1, device_id=across, device_id_type=MESH)
    pl.semaphore_signal(barrier, 1, device_id=partner, device_id_type=MESH)
    for k in range(1, nx):
        pl.semaphore_signal(
            barrier, 1, device_id={"tp": ((x + k) % nx) * 2 + c}, device_id_type=MESH
        )
    pl.semaphore_wait(barrier, (n - 1) + 2 + (nx - 1))

    units = w_down.shape[0] // 32
    first = units // 2
    second = (units - first + 1) // 2
    ends = (0, first * 32, (first + second) * 32, w_down.shape[0])
    streams = (
        (w_uv, uv_buf, 0, w_uv.shape[0]),
        (w_mix, mix_buf, 0, w_mix.shape[0]),
        (w_gate, gate_buf, 0, w_gate.shape[0]),
        (w_up, up_buf, 0, w_up.shape[0]),
    ) + tuple((w_down, down_buf, ends[q], ends[q + 1] - ends[q]) for q in range(3))
    UV, MIX, GATE, UP, DOWN_A, DOWN_B, DOWN_C = range(7)

    def part(k, who):
        half = streams[k][3] // 2
        return pl.ds(pl.multiple_of(streams[k][2] + who * half, 16), half)

    def z_copy(k, j, step, own):
        src, buf = streams[k][:2]
        sl = part(k, g)
        dst = buf.at[j, sl, :]
        slot = n if (own and step < 0) else j
        return remote(
            src.at[sl, :] if own else dst,
            dst,
            z_send.at[k, slot],
            z_recv.at[k, j],
            {"fs": jnp.clip(i + step, 0, n - 1)},
        )

    def y_copy(k, j, who):
        dst = streams[k][1].at[j, part(k, who), :]
        return remote(dst, dst, y_send.at[k, j], y_recv.at[k, j], across)

    def local_copy(k):
        src, buf, r0, count = streams[k]
        sl = pl.ds(r0, count)
        return pltpu.make_async_copy(src.at[sl, :], buf.at[i, sl, :], w_local.at[k])

    def own(k):
        @pl.when(i + 1 < n)
        def _():
            z_copy(k, i, 1, True).start()

        @pl.when(i > 0)
        def _():
            z_copy(k, i, -1, True).start()

    def service(k, s):
        left, right = i - s, i + s

        @pl.when(left >= 0)
        def _():
            z_copy(k, left, 1, False).wait_recv()

            @pl.when(i + 1 < n)
            def _():
                z_copy(k, left, 1, False).start()

            y_copy(k, left, g).start()

        @pl.when(right < n)
        def _():
            z_copy(k, right, -1, False).wait_recv()

            @pl.when(i > 0)
            def _():
                z_copy(k, right, -1, False).start()

            y_copy(k, right, g).start()

    def run(k, begin, end):
        for s in range(begin, min(end, n)):
            service(k, s)

    def finish(k):
        local_copy(k).wait()
        for s in range(1, n):
            y_copy(k, lax.rem(i + s, n), 1 - g).wait_recv()

    def drain(k):
        @pl.when(i + 1 < n)
        def _():
            z_copy(k, i, 1, True).wait_send()

        @pl.when(i > 0)
        def _():
            z_copy(k, i, -1, True).wait_send()

        for s in range(1, n):
            j = lax.rem(i + s, n)
            y_copy(k, j, g).wait_send()

            @pl.when(jnp.logical_and(j < i, i + 1 < n))
            def _():
                z_copy(k, j, 1, False).wait_send()

            @pl.when(jnp.logical_and(j > i, i > 0))
            def _():
                z_copy(k, j, -1, False).wait_send()

    def scale_copy(s, mine):
        j = i if mine else lax.rem(i + s, n)
        return remote(
            scales,
            scale_buf.at[j],
            s_send.at[s],
            s_recv.at[j],
            {"fs": lax.rem(i + s, n)},
        )

    def chunk(h):
        return pl.ds(h * rt, rt)

    def far(k):
        return lax.rem(x + k, nx)

    def ag_x(r, src, buf, k, h):
        return remote(
            src.at[chunk(h), :],
            buf.at[t, chunk(h), :],
            g_send.at[r, k, h],
            g_recv.at[r, t, h],
            {"tp": far(k) * 2 + c} if k else partner,
        )

    def ag_in(r, buf, slot, h):
        ref = buf.at[slot, chunk(h), :]
        return remote(ref, ref, g_fwd.at[r, 0, h], g_recv.at[r, slot, h], partner)

    def ag_fwd(r, buf, k, h):
        slot = far(k) * 2 + c
        ref = buf.at[slot, chunk(h), :]
        return remote(ref, ref, g_fwd.at[r, k, h], g_recv.at[r, slot, h], partner)

    def ag_local(r, src, buf):
        return pltpu.make_async_copy(src, buf.at[t], g_local.at[r])

    def ag_start(r, src, buf):
        for h in range(H):
            for k in list(range(1, nx)) + [0]:
                ag_x(r, src, buf, k, h).start()
        ag_local(r, src, buf).start()

    def ag_finish(r, src, buf):
        for h in range(H):
            for k in range(1, nx):
                ag_fwd(r, buf, k, h).wait_recv()
                ag_fwd(r, buf, k, h).start()
        for h in range(H):
            for k in range(nx):
                ag_in(r, buf, far(k) * 2 + 1 - c, h).wait_recv()
        ag_local(r, src, buf).wait()

    def ag_drain(r, src, buf):
        for h in range(H):
            for k in range(nx):
                ag_x(r, src, buf, k, h).wait_send()
            for k in range(1, nx):
                ag_fwd(r, buf, k, h).wait_send()

    def norm(buf, gain):
        tile = 128

        def body(b, carry):
            sl = pl.ds(pl.multiple_of(b * tile, tile), tile)
            total = jnp.zeros((tile, 1), jnp.float32)
            for q in range(n_tp):
                wide = buf[q, sl, :].astype(jnp.float32)
                total = total + jnp.sum(wide * wide, axis=1, keepdims=True)
            factor = lax.rsqrt(total / (n_tp * dt) + eps)
            for q in range(n_tp):
                cols = slice(q * dt, (q + 1) * dt)
                wide = buf[q, sl, :].astype(jnp.float32)
                normed[sl, cols] = (wide * factor * gain[:, cols]).astype(jnp.bfloat16)
            return carry

        lax.fori_loop(0, rows // tile, body, 0)

    def pair_copy(r, xo, h):
        return remote(
            give_buf.at[xo, chunk(h), :],
            pair_buf.at[r, xo, chunk(h), :],
            p_send.at[r, xo, h],
            p_recv.at[r, xo, h],
            partner,
        )

    def far_copy(r, xo, h, slot):
        return remote(
            send_buf.at[xo, chunk(h), :],
            far_buf.at[r, slot, chunk(h), :],
            f_send.at[r, xo, h],
            f_recv.at[r, slot, h],
            {"tp": xo * 2 + c},
        )

    def reduce_over_tp(r, hidden, buf, scale_row, hook):
        def partial(owner, h):
            ws = [buf[owner * per + q] for q in range(per)]
            ss = [scale_buf[owner * per + q, scale_row : scale_row + 1, :] for q in range(per)]
            w = ws[0] if per == 1 else jnp.concatenate(ws, axis=1)
            s = ss[0] if per == 1 else jnp.concatenate(ss, axis=1)
            return jnp.dot(hidden[chunk(h), :], w, preferred_element_type=jnp.float32) * s

        for k in range(1, nx + 1):
            xo = far(k)
            for h in range(H):
                give_buf[xo, chunk(h), :] = partial(xo * 2 + 1 - c, h).astype(jnp.bfloat16)
                keep[xo, chunk(h), :] = partial(xo * 2 + c, h)
                pair_copy(r, xo, h).start()
            for h in range(H):
                pair_copy(r, xo, h).wait_recv()
                both = keep[xo, chunk(h), :] + pair_buf[r, xo, chunk(h), :].astype(jnp.float32)
                if k < nx:
                    send_buf[xo, chunk(h), :] = both.astype(jnp.bfloat16)
                else:
                    keep[xo, chunk(h), :] = both
            if k < nx:
                for h in range(H):
                    far_copy(r, xo, h, x).start()
        hook()

    def reduced(r, h):
        total = keep[x, chunk(h), :]
        for k in range(1, nx):
            far_copy(r, far(k), h, far(k)).wait_recv()
            total = total + far_buf[r, far(k), chunk(h), :].astype(jnp.float32)
        return total

    def reduce_drain(r):
        for k in range(1, nx + 1):
            for h in range(H):
                pair_copy(r, far(k), h).wait_send()
                if k < nx:
                    far_copy(r, far(k), h, x).wait_send()

    own(UV)
    own(MIX)
    ag_start(0, tokens, tok_buf)
    for s in range(1, n):
        scale_copy(s, True).start()
    own_scale = pltpu.make_async_copy(scales, scale_buf.at[i], s_local)
    own_scale.start()
    for k in range(7):
        local_copy(k).start()
    for s in range(1, n):
        service(UV, s)
        service(MIX, s)
        if s == max(n - 2, 1):
            own(GATE)
            own(UP)
    ag_finish(0, tokens, tok_buf)
    norm(tok_buf, gains[0:1, :])
    own_scale.wait()
    for s in range(1, n):
        scale_copy(s, False).wait_recv()
    finish(UV)

    groups, span = spatial.shape[0], spatial.shape[1]
    width = uv_scale.shape[1]
    wide = width // groups
    causal = lax.broadcasted_iota(jnp.int32, (span, span), 0) >= lax.broadcasted_iota(
        jnp.int32, (span, span), 1
    )
    uv_w = uv_buf[...].reshape(-1, 2 * width)
    tilt = [jnp.broadcast_to(bias[q : q + 1, :], (span, span)).T[:, :1] for q in range(groups)]
    for h in range(H):
        pre = jnp.dot(normed[chunk(h), :], uv_w, preferred_element_type=jnp.float32)
        u = gelu(pre[:, :width] * uv_scale[0:1, :])
        v = gelu(pre[:, width:] * uv_scale[1:2, :]).astype(jnp.bfloat16)
        for q in range(groups):
            m = jnp.where(causal, spatial[q].astype(jnp.float32), 0.0).astype(jnp.bfloat16)
            cols = slice(q * wide, (q + 1) * wide)
            for b in range(rt // span):
                sl = slice(b * span, (b + 1) * span)
                mixed = jnp.dot(m, v[sl, cols], preferred_element_type=jnp.float32)
                mixed = mixed + tilt[q]
                gated[h * rt + b * span : h * rt + (b + 1) * span, cols] = (
                    u[sl, cols] * mixed
                ).astype(jnp.bfloat16)
    finish(MIX)

    def after_mix():
        service(GATE, 1)
        own(DOWN_A)

    reduce_over_tp(0, gated, mix_buf, 0, after_mix)
    for h in range(H):
        resid[chunk(h), :] = (
            tokens[chunk(h), :].astype(jnp.float32) + reduced(0, h)
        ).astype(jnp.bfloat16)
    ag_start(1, resid, res_buf)
    reduce_drain(0)
    run(UP, 1, 2)
    run(GATE, 2, 3)
    own(DOWN_B)
    ag_finish(1, resid, res_buf)
    norm(res_buf, gains[1:2, :])
    run(UP, 2, 3)
    run(GATE, 3, n)
    own(DOWN_C)
    run(DOWN_A, 1, 2)
    run(DOWN_B, 1, 2)
    finish(GATE)


    ff = ffn_scale.shape[1]
    gt = rows // 4

    def gate_step(b, carry):
        sl = pl.ds(pl.multiple_of(b * gt, 64), gt)
        a = jnp.dot(
            normed[sl, :], gate_buf[...].reshape(-1, ff), preferred_element_type=jnp.float32
        )
        a = a * ffn_scale[0:1, :]
        silu_buf[sl, :] = a / (1.0 + jnp.exp(-a))
        return carry

    lax.fori_loop(0, 4, gate_step, 0)
    run(UP, 3, n)
    run(DOWN_C, 1, 2)
    run(DOWN_A, 2, 3)
    run(DOWN_B, 2, 3)
    finish(UP)

    def up_step(b, carry):
        sl = pl.ds(pl.multiple_of(b * gt, 64), gt)
        a = jnp.dot(
            normed[sl, :], up_buf[...].reshape(-1, ff), preferred_element_type=jnp.float32
        )
        act[sl, :] = (silu_buf[sl, :] * (a * ffn_scale[1:2, :])).astype(jnp.bfloat16)
        return carry

    lax.fori_loop(0, 4, up_step, 0)
    run(DOWN_C, 2, 3)
    run(DOWN_A, 3, n)
    run(DOWN_B, 3, n)
    run(DOWN_C, 3, n)
    finish(DOWN_A)
    finish(DOWN_B)
    finish(DOWN_C)
    reduce_over_tp(1, act, down_buf, 8, lambda: None)
    for h in range(H):
        out[chunk(h), :] = (
            resid[chunk(h), :].astype(jnp.float32) + reduced(1, h)
        ).astype(jnp.bfloat16)
    reduce_drain(1)
    ag_drain(0, tokens, tok_buf)
    ag_drain(1, resid, res_buf)
    for k in range(7):
        drain(k)
    for s in range(1, n):
        scale_copy(s, True).wait_send()


def local(
    dims,
    tokens,
    mix_gain,
    w_u,
    w_v,
    u_scale,
    v_scale,
    spatial,
    spatial_bias,
    w_mix,
    mix_scale,
    ffn_gain,
    w_gate,
    w_up,
    gate_scale,
    up_scale,
    w_down,
    down_scale,
):
    n, n_tp = dims
    nx = n_tp // 2
    half = jnp.bfloat16
    rows, dt = tokens.shape
    df = mix_scale.shape[1]
    scales = jnp.concatenate(
        [jnp.broadcast_to(mix_scale, (8, df)), jnp.broadcast_to(down_scale, (8, df))], axis=0
    )
    w_uv = jnp.concatenate([w_u, w_v], axis=1).astype(half)
    hbm = pl.BlockSpec(memory_space=pl.ANY)
    vmem = pl.BlockSpec(memory_space=pltpu.VMEM)
    ff = w_gate.shape[1]
    dma = pltpu.SemaphoreType.DMA
    return pl.pallas_call(
        functools.partial(layer_kernel, dims),
        out_shape=jax.ShapeDtypeStruct((rows, dt), half),
        in_specs=[vmem, vmem] + [hbm] * 5 + [vmem] * 5,
        out_specs=vmem,
        scratch_shapes=[
            pltpu.VMEM((n,) + w_uv.shape, half),
            pltpu.VMEM((n,) + w_mix.shape, half),
            pltpu.VMEM((n,) + w_gate.shape, half),
            pltpu.VMEM((n,) + w_up.shape, half),
            pltpu.VMEM((n,) + w_down.shape, half),
            pltpu.VMEM((n,) + scales.shape, jnp.float32),
            pltpu.VMEM((n_tp, rows, dt), half),
            pltpu.VMEM((n_tp, rows, dt), half),
            pltpu.VMEM((rows, n_tp * dt), half),
            pltpu.VMEM((rows, w_u.shape[1]), half),
            pltpu.VMEM((rows, ff), jnp.float32),
            pltpu.VMEM((rows, ff), half),
            pltpu.VMEM((rows, dt), half),
            pltpu.VMEM((nx, rows, dt), half),
            pltpu.VMEM((nx, rows, dt), half),
            pltpu.VMEM((2, nx, rows, dt), half),
            pltpu.VMEM((2, nx, rows, dt), half),
            pltpu.VMEM((nx, rows, dt), jnp.float32),
            dma((7, n + 1)),
            dma((7, n)),
            dma((7, n)),
            dma((7, n)),
            dma((7,)),
            dma((n,)),
            dma((n,)),
            dma,
            dma((2, nx, H)),
            dma((2, nx, H)),
            dma((2, n_tp, H)),
            dma((2,)),
            dma((2, nx, H)),
            dma((2, nx, H)),
            dma((2, nx, H)),
            dma((2, nx, H)),
        ],
        compiler_params=pltpu.CompilerParams(
            collective_id=0, has_side_effects=True, vmem_limit_bytes=66000000
        ),
    )(
        tokens,
        jnp.stack([mix_gain, ffn_gain]),
        w_uv,
        w_mix.astype(half),
        w_gate.astype(half),
        w_up.astype(half),
        w_down.astype(half),
        jnp.stack([u_scale, v_scale]),
        spatial,
        spatial_bias,
        scales,
        jnp.stack([gate_scale, up_scale]),
    )


def solution(mesh):
    placed = (
        P(("grp", "fs"), "tp"),
        P(),
        P("fs", "tp"),
        P("fs", "tp"),
        P("tp"),
        P("tp"),
        P("tp", None, None),
        P("tp", None),
        P("tp", "fs"),
        P(None, "fs"),
        P(),
        P("fs", "tp"),
        P("fs", "tp"),
        P("tp"),
        P("tp"),
        P("tp", "fs"),
        P(None, "fs"),
    )
    dims = (mesh.shape["fs"], mesh.shape["tp"])
    return jax.shard_map(
        functools.partial(local, dims),
        mesh=mesh,
        in_specs=placed,
        out_specs=P(("grp", "fs"), "tp"),
        check_vma=False,
    )
```

profile of v0, /device:TPU:0, one launch (start us, length us, event | category | flops | bytes accessed | tf_op | source)
XLA Modules:
  0.0 242.0 jit_solution(8783871315519701852)
XLA Ops:
  0.0 0.0 copy-start
  0.0 1.4 pad_maximum_fusion.4.uv_scale
  1.4 0.7 stack.33
  2.1 0.7 stack.34
  2.8 0.6 pad_maximum_fusion.3.ffn_scale
  3.4 1.3 pad_maximum_fusion.2.gains
  4.8 0.7 broadcast_in_dim.15
  5.4 0.7 broadcast_in_dim.17
  6.1 0.6 pad_maximum_fusion.1.scales
  6.7 1.1 convert.6
  7.8 1.1 convert.7
  8.9 0.0 copy-start.1
  8.9 0.8 pad_maximum_fusion.w_uv
  9.7 2.0 convert_element_type.13.w_mix
  11.7 0.0 copy-done
  11.7 1.3 convert_element_type.14.w_gate
  13.0 0.0 copy-done.1
  13.0 0.0 copy-start.2
  13.0 1.3 convert_element_type.15.w_up
  14.3 1.1 copy-done.2
  15.3 1.3 convert_element_type.16.w_down
  16.7 223.2 %shard_map.163 = bf16[768,512]{1,0:T(8,128)(2,1)} custom-call(bf16[768,512]{1,0:T(8,128)(2,1)} %tokens.1, f32[2,2048]{1,0:T(2,128)} %pad_maximum_fusion.2.gains, bf16[512,512]{1,0:T(8,128)(2,1)} %pad_maximum_fusion.w_uv, bf16[256,512]{1,0:T(8,128)(2,1)} %convert_element_type.13.w_mix, bf16[512,1408]{1,0:T(8,128)(2,1)} %convert_element_type.14.w_gate, ...), custom_call_target="tpu_custom_call" | custom-call | tf_op jit(solution)/shard_map/pallas_call | solution.py:492
  239.9 2.1 copy.19
Async XLA Ops:
  0.0 11.7 %copy-start = (f32[512,1408]{1,0:T(8,128)S(1)}, f32[512,1408]{1,0:T(8,128)}, u32[]{:S(2)}) copy-start(f32[512,1408]{1,0:T(8,128)} %param.28) | copy-start | bytes 8650756
  8.9 4.1 %copy-start.1 = (f32[512,1408]{1,0:T(8,128)S(1)}, f32[512,1408]{1,0:T(8,128)}, u32[]{:S(2)}) copy-start(f32[512,1408]{1,0:T(8,128)} %param.29) | copy-start | bytes 8650756
  13.0 2.3 copy-start.2
where the time goes:
time: 243 us; the launch traced here: 242 us
  Pallas kernels  223 us (92%)
  other arithmetic  12.8 us (5%)
  local copies, waits for them, and re-layouts  5.92 us (2%)
    pallas_call x1, Pallas kernels, local(): pl.pallas_call(functools.partial(layer_kernel, dims), out_shape=jax.Shape...  223 us

commit v1 on v0

v1 whole, which is shorter than its diff:
```python
import functools

import jax
import jax.numpy as jnp
from jax import lax
from jax.experimental import pallas as pl
from jax.experimental.pallas import tpu as pltpu
from jax.sharding import PartitionSpec as P

MESH = pl.DeviceIdType.MESH
eps = 1e-06
H = 2
C = 4
half_root = 0.7071067811865476
f32 = jnp.float32
bf16 = jnp.bfloat16


def gelu(a):
    return 0.5 * a * (1.0 + lax.erf(a * half_root))


def up_to(a, b):
    return -(-a // b) * b


def layer_kernel(
    dims,
    tokens,
    mix_gain,
    ffn_gain,
    w_u,
    w_v,
    w_mix,
    w_gate,
    w_up,
    w_down,
    u_scale,
    v_scale,
    spatial,
    bias,
    mix_scale,
    gate_scale,
    up_scale,
    down_scale,
    out,
    uv_stage,
    mix_stage,
    gate_stage,
    up_stage,
    uv_buf,
    mix_buf,
    gate_buf,
    up_buf,
    down_buf,
    tok_buf,
    res_buf,
    gated,
    silu_buf,
    act,
    give_buf,
    pair_buf,
    keep,
    send_buf,
    far_buf,
    load_sem,
    z_send,
    z_recv,
    y_send,
    y_recv,
    a_send,
    a_fwd,
    a_recv,
    gx_send,
    gz_send,
    gd_send,
    gfz_send,
    gfx_send,
    g_recv,
    p_send,
    p_recv,
    m_send,
    m_recv,
    f_send,
    f_recv,
):
    n, n_tp, parts = dims
    nx = n_tp // 2
    i = lax.axis_index("fs")
    g = lax.axis_index("grp")
    t = lax.axis_index("tp")
    x, c = t // 2, t % 2
    m = i % 2
    rows, dt = tokens.shape
    dr, ff = w_gate.shape
    df = w_down.shape[1]
    per = dt // df
    rt = rows // H
    ct = rows // C
    wide = gate_buf.shape[2]
    rest = ff - wide
    padded = up_to(rest, 128)
    widths = (wide, padded)
    heights = (wide, rest)
    partner = {"tp": x * 2 + 1 - c}
    across = {"grp": 1 - g}
    beside = {"fs": i + 1 - 2 * m}

    def far(k):
        return lax.rem(x + k, nx)

    def far_id(k):
        return {"tp": far(k) * 2 + c}

    def remote(src, dst, ss, rs, device):
        return pltpu.make_async_remote_copy(
            src_ref=src,
            dst_ref=dst,
            send_sem=ss,
            recv_sem=rs,
            device_id=device,
            device_id_type=MESH,
        )

    width = w_u.shape[1]
    loads = [
        pltpu.make_async_copy(w_u, uv_stage.at[0], load_sem.at[0]),
        pltpu.make_async_copy(w_v, uv_stage.at[1], load_sem.at[1]),
        pltpu.make_async_copy(w_mix, mix_stage, load_sem.at[2]),
        pltpu.make_async_copy(w_gate, gate_stage, load_sem.at[3]),
        pltpu.make_async_copy(w_up, up_stage, load_sem.at[4]),
        pltpu.make_async_copy(w_down, silu_buf.at[pl.ds(0, ff), pl.ds(0, df)], load_sem.at[5]),
        pltpu.make_async_copy(tokens, tok_buf.at[t], load_sem.at[6]),
    ]
    for copy in loads:
        copy.start()

    barrier = pltpu.get_barrier_semaphore()
    for k in range(1, n):
        pl.semaphore_signal(barrier, 1, device_id={"fs": (i + k) % n}, device_id_type=MESH)
    pl.semaphore_signal(barrier, 1, device_id=across, device_id_type=MESH)
    pl.semaphore_signal(barrier, 1, device_id=partner, device_id_type=MESH)
    for k in range(1, nx):
        pl.semaphore_signal(barrier, 1, device_id=far_id(k), device_id_type=MESH)
    pl.semaphore_wait(barrier, (n - 1) + 2 + (nx - 1))

    UV, MIX, GATE, UP, DOWN = range(5)
    bufs = (uv_buf, mix_buf, gate_buf, up_buf) + (down_buf,) * parts
    streams = len(bufs)
    dc = df // parts

    def view(k, slot, who, h):
        ref = bufs[k]
        if k < GATE:
            count = ref.shape[1] // 2
            return ref.at[slot, pl.ds(pl.multiple_of(who * count, 16), count), :]
        if k < DOWN:
            count = dr // 2
            sl = pl.ds(pl.multiple_of(who * count, 16), count)
            return ref.at[slot, sl, pl.ds(0, widths[h])]
        count = heights[h] // 2
        sl = pl.ds(pl.multiple_of(who * count, 16), count)
        return ref.at[slot, sl, pl.ds((k - DOWN) * dc, dc)]

    def z_copy(k, src, dst, step, h, sem):
        return remote(
            view(k, src, g, h),
            view(k, dst, g, h),
            z_send.at[k, sem],
            z_recv.at[k, dst],
            {"fs": jnp.clip(i + step, 0, n - 1)},
        )

    def y_copy(k, j, who, h):
        ref = view(k, j, who, h)
        return remote(ref, ref, y_send.at[k, j], y_recv.at[k, j], across)

    def by_half(k, f):
        if k < GATE:
            f(0)
            return
        for h in range(2):

            @pl.when(m == h)
            def _():
                f(h)

    def own_each(k, act_on):
        stride = 1 if k < GATE else 2

        def each(h):
            if k >= GATE:

                @pl.when(i + 1 < n)
                def _():
                    act_on(z_copy(k, n, i, 1, 1 - h, n + 2))

                @pl.when(i > 0)
                def _():
                    act_on(z_copy(k, n, i, -1, 1 - h, n + 3))

            @pl.when(i + stride < n)
            def _():
                act_on(z_copy(k, i, i, stride, h, n))

            @pl.when(i - stride >= 0)
            def _():
                act_on(z_copy(k, i, i, -stride, h, n + 1))

        by_half(k, each)

    def own(k):
        own_each(k, lambda copy: copy.start())

    def service(k, s):
        if s >= n:
            return
        stride = 1 if k < GATE else 2

        def each(h):
            left, right = i - s, i + s

            @pl.when(left >= 0)
            def _():
                z_copy(k, left, left, stride, h, left).wait_recv()

                @pl.when(i + stride < n)
                def _():
                    z_copy(k, left, left, stride, h, left).start()

                y_copy(k, left, g, h).start()

            @pl.when(right < n)
            def _():
                z_copy(k, right, right, -stride, h, right).wait_recv()

                @pl.when(i - stride >= 0)
                def _():
                    z_copy(k, right, right, -stride, h, right).start()

                y_copy(k, right, g, h).start()

        by_half(k, each)

    def run(k, begin, end):
        for s in range(begin, end):
            service(k, s)

    def finish(k):
        def each(h):
            for s in range(1, n):
                y_copy(k, lax.rem(i + s, n), 1 - g, h).wait_recv()

        by_half(k, each)

    def drain(k):
        stride = 1 if k < GATE else 2
        own_each(k, lambda copy: copy.wait_send())

        def each(h):
            for s in range(1, n):
                j = lax.rem(i + s, n)
                y_copy(k, j, g, h).wait_send()

                @pl.when(jnp.logical_and(j < i, i + stride < n))
                def _():
                    z_copy(k, j, j, stride, h, j).wait_send()

                @pl.when(jnp.logical_and(j > i, i - stride >= 0))
                def _():
                    z_copy(k, j, j, -stride, h, j).wait_send()

        by_half(k, each)

    def chunk(h):
        return pl.ds(h * rt, rt)

    def ag_x(k, h):
        return remote(
            tokens.at[chunk(h), :],
            tok_buf.at[t, chunk(h), :],
            a_send.at[k, h],
            a_recv.at[t, h],
            far_id(k) if k else partner,
        )

    def ag_fwd(k, h):
        slot = far(k) * 2 + c
        ref = tok_buf.at[slot, chunk(h), :]
        return remote(ref, ref, a_fwd.at[k, h], a_recv.at[slot, h], partner)

    def ag_in(k, h):
        slot = far(k) * 2 + 1 - c
        ref = tok_buf.at[slot, chunk(h), :]
        return remote(ref, ref, a_fwd.at[0, h], a_recv.at[slot, h], partner)

    def rchunk(q):
        return pl.ds(q * ct, ct)

    def block(e, slot, q):
        return res_buf.at[e, slot, rchunk(q), :]

    def gx(k, q):
        return remote(block(0, t, q), block(0, t, q), gx_send.at[k, q], g_recv.at[0, t, q], far_id(k))

    def gz(q):
        return remote(block(0, t, q), block(1, t, q), gz_send.at[q], g_recv.at[1, t, q], beside)

    def gd(e, k, q):
        slot = far(k) * 2 + c
        ref = block(e, slot, q)
        return remote(ref, ref, gd_send.at[e, k, q], g_recv.at[e, slot, q], partner)

    def gd_in(e, k, q):
        slot = far(k) * 2 + 1 - c
        ref = block(e, slot, q)
        return remote(ref, ref, gd_send.at[e, k, q], g_recv.at[e, slot, q], partner)

    def gfz(k, q):
        slot = far(k) * 2 + c
        return remote(
            block(0, slot, q), block(1, slot, q), gfz_send.at[k, q], g_recv.at[1, slot, q], beside
        )

    def gfx(k, q):
        return remote(block(1, t, q), block(1, t, q), gfx_send.at[k, q], g_recv.at[1, t, q], far_id(k))

    def g_start(q):
        for k in range(1, nx):
            gx(k, q).start()
        gz(q).start()
        gd(0, 0, q).start()

    def g_first(q):
        for k in range(1, nx):
            gd(0, k, q).wait_recv()
            if q < C // 2:
                gfz(k, q).start()
            gd(0, k, q).start()
        gd(1, 0, q).wait_recv()
        if q >= C // 2:
            for k in range(1, nx):
                gfx(k, q).start()
        gd(1, 0, q).start()

    def g_second(q):
        for k in range(1, nx):
            gd(1, k, q).wait_recv()
            gd(1, k, q).start()

    def g_ready(e, q):
        for k in range(nx):
            gd_in(e, k, q).wait_recv()

    def g_drain():
        for q in range(C):
            gz(q).wait_send()
            for e in range(2):
                for k in range(nx):
                    gd(e, k, q).wait_send()
            for k in range(1, nx):
                gx(k, q).wait_send()
                if q < C // 2:
                    gfz(k, q).wait_send()
                else:
                    gfx(k, q).wait_send()

    bw = dt // parts

    def weight(buf, owner, p):
        ws = [buf[owner * per + q, :, p * dc : (p + 1) * dc] for q in range(per)]
        return ws[0] if per == 1 else jnp.concatenate(ws, axis=1)

    def pair_copy(r, p, xo, e, h):
        return remote(
            give_buf.at[p, xo, e, h],
            pair_buf.at[p, xo, e, h],
            p_send.at[r, p, xo, e, h],
            p_recv.at[r, p, xo, e, h],
            partner,
        )

    def partials(r, p, xo, e, h, left, buf):
        give_buf[p, xo, e, h] = jnp.dot(
            left, weight(buf, xo * 2 + 1 - c, p), preferred_element_type=f32
        ).astype(bf16)
        pair_copy(r, p, xo, e, h).start()
        keep[p, xo, e, h] = jnp.dot(left, weight(buf, xo * 2 + c, p), preferred_element_type=f32)

    def both(r, p, xo, e, h):
        pair_copy(r, p, xo, e, h).wait_recv()
        return keep[p, xo, e, h] + pair_buf[p, xo, e, h].astype(f32)

    def mix_copy(p, k, h, slot):
        xo = far(k)
        return remote(
            send_buf.at[p, xo, 0, h],
            far_buf.at[p, slot, 0, h],
            m_send.at[p, xo, h],
            m_recv.at[p, slot, h],
            far_id(k),
        )

    def far_copy(p, src, dst, device):
        return remote(
            send_buf.at[(p,) + src],
            far_buf.at[(p,) + dst],
            f_send.at[(p,) + src],
            f_recv.at[(p,) + dst],
            device,
        )

    def x_one(p, k, e):
        return far_copy(p, (far(k), e, 0), (x, e, 0), far_id(k))

    def x_one_in(p, k, e):
        return far_copy(p, (far(k), e, 0), (far(k), e, 0), far_id(k))

    def z_one(p, k):
        return far_copy(p, (far(k), 1, 1), (far(k), 0, 1), beside)

    def z_two(p):
        return far_copy(p, (x, 1, 0), (x, 0, 0), beside)

    def x_two(p, k):
        return far_copy(p, (far(k), 0, 1), (x, 1, 1), far_id(k))

    def x_two_in(p, k):
        return far_copy(p, (far(k), 0, 1), (far(k), 1, 1), far_id(k))

    def arrived(p, a, e, h):
        return far_buf[p, a, e, h].astype(f32)

    def factor(rows_in):
        total = jnp.zeros((rows_in.shape[0], 1), f32)
        for q in range(n_tp):
            part = rows_in[:, q * dt : (q + 1) * dt].astype(f32)
            total = total + jnp.sum(part * part, axis=1, keepdims=True)
        return lax.rsqrt(total / (n_tp * dt) + eps)

    def column(gain, s):
        lanes = gain[0:1, pl.ds(pl.multiple_of(i * dr + s * 128, 128), 128)]
        return jnp.broadcast_to(lanes, (128, 128)).T[:, :1]

    for h in range(H):
        for k in list(range(1, nx)) + [0]:
            ag_x(k, h).start()
    loads[0].wait()
    loads[1].wait()
    for s in range(dr // 128):
        sl = slice(s * 128, (s + 1) * 128)
        gain = column(mix_gain, s)
        uv_buf[i, sl, :width] = (uv_stage[0, sl, :] * gain * u_scale[0:1, :]).astype(bf16)
        uv_buf[i, sl, width:] = (uv_stage[1, sl, :] * gain * v_scale[0:1, :]).astype(bf16)
    own(UV)
    loads[2].wait()
    mix_buf[i] = (mix_stage[...] * mix_scale[0:1, :]).astype(bf16)
    own(MIX)

    def cast_in(stage, scale, buf):
        for s in range(dr // 128):
            sl = slice(s * 128, (s + 1) * 128)
            gain = column(ffn_gain, s)
            for h, (lo, hi) in enumerate(((0, wide), (wide, ff))):
                slot = jnp.where(m == h, i, n)
                buf[slot, sl, : hi - lo] = (
                    stage[sl, lo:hi] * gain * scale[0:1, lo:hi]
                ).astype(bf16)
                if hi - lo < widths[h]:
                    buf[slot, sl, hi - lo : widths[h]] = jnp.zeros(
                        (128, widths[h] - hi + lo), bf16
                    )

    loads[3].wait()
    cast_in(gate_stage, gate_scale, gate_buf)
    loads[4].wait()
    cast_in(up_stage, up_scale, up_buf)
    loads[5].wait()
    for h, (lo, hi) in enumerate(((0, wide), (wide, ff))):
        slot = jnp.where(m == h, i, n)
        down_buf[slot, : hi - lo, :] = (silu_buf[lo:hi, :df] * down_scale[0:1, :]).astype(bf16)

    @pl.when(m == 1)
    def _():
        for j in range(n):
            if padded < wide:
                gate_buf[j, :, padded:] = jnp.zeros((dr, wide - padded), bf16)
                up_buf[j, :, padded:] = jnp.zeros((dr, wide - padded), bf16)
            down_buf[j, rest:, :] = jnp.zeros((wide - rest, df), bf16)

    for s in range(1, n):
        service(UV, s)
        service(MIX, s)
        if s == max(n - 2, 1):
            own(GATE)
    for h in range(H):
        for k in range(1, nx):
            ag_fwd(k, h).wait_recv()
            ag_fwd(k, h).start()
    for h in range(H):
        for k in range(nx):
            ag_in(k, h).wait_recv()
    loads[6].wait()
    finish(UV)

    groups, span = spatial.shape[0], spatial.shape[1]
    lanes = width // groups
    causal = lax.broadcasted_iota(jnp.int32, (span, span), 0) >= lax.broadcasted_iota(
        jnp.int32, (span, span), 1
    )
    tilt = [jnp.broadcast_to(bias[q : q + 1, :], (span, span)).T[:, :1] for q in range(groups)]

    def gather_rows(pieces):
        return jnp.concatenate(pieces, axis=1)

    for h in range(H):
        left = gather_rows([tok_buf[q, chunk(h), :] for q in range(n_tp)])
        pre = jnp.dot(left, uv_buf[...].reshape(-1, 2 * width), preferred_element_type=f32)
        pre = pre * factor(left)
        u = gelu(pre[:, :width])
        v = gelu(pre[:, width:]).astype(bf16)
        for q in range(groups):
            mat = jnp.where(causal, spatial[q].astype(f32), 0.0).astype(bf16)
            cols = slice(q * lanes, (q + 1) * lanes)
            for b in range(rt // span):
                sl = slice(b * span, (b + 1) * span)
                mixed = jnp.dot(mat, v[sl, cols], preferred_element_type=f32) + tilt[q]
                gated[h * rt + b * span : h * rt + (b + 1) * span, cols] = (
                    u[sl, cols] * mixed
                ).astype(bf16)
    finish(MIX)

    for k in range(1, nx):
        for h in range(H):
            for p in range(parts):
                partials(0, p, far(k), 0, h, gated[chunk(h), :], mix_buf)
        for h in range(H):
            for p in range(parts):
                send_buf[p, far(k), 0, h] = both(0, p, far(k), 0, h).astype(bf16)
                mix_copy(p, k, h, x).start()
    service(GATE, 1)
    own(UP)
    for h in range(H):
        for p in range(parts):
            partials(0, p, x, 0, h, gated[chunk(h), :], mix_buf)
    service(GATE, 2)
    for h in range(H):
        for p in range(parts):
            total = both(0, p, x, 0, h)
            for k in range(1, nx):
                mix_copy(p, k, h, far(k)).wait_recv()
                total = total + arrived(p, far(k), 0, h)
            cols = slice(p * bw, (p + 1) * bw)
            res_buf[0, t, chunk(h), cols] = (
                tok_buf[t, chunk(h), cols].astype(f32) + total
            ).astype(bf16)
        for q in range(h * (C // H), (h + 1) * (C // H)):
            g_start(q)
    run(GATE, 3, n)
    service(UP, 1)
    g_first(0)
    g_first(1)
    service(UP, 2)
    for k in range(parts):
        own(DOWN + k)
    g_first(2)
    g_first(3)
    finish(GATE)

    def gate_tiles(e, begin, end):
        def body(b, carry):
            sl = pl.ds(pl.multiple_of(b * ct, 64), ct)
            left = gather_rows([res_buf[e, q, sl, :] for q in range(n_tp)])
            inv = factor(left)
            a = jnp.dot(left, gate_buf[:n].reshape(-1, wide), preferred_element_type=f32) * inv
            silu_buf[pl.ds(pl.multiple_of(e * rows + b * ct, 64), ct), :] = (
                a / (1.0 + jnp.exp(-a)) * inv
            )
            return carry

        lax.fori_loop(begin, end, body, 0)

    def up_tiles(e):
        def body(b, carry):
            sl = pl.ds(pl.multiple_of(b * ct, 64), ct)
            flat = pl.ds(pl.multiple_of(e * rows + b * ct, 64), ct)
            left = gather_rows([res_buf[e, q, sl, :] for q in range(n_tp)])
            a = jnp.dot(left, up_buf[:n].reshape(-1, wide), preferred_element_type=f32)
            act[flat, :] = (silu_buf[flat, :] * a).astype(bf16)
            return carry

        lax.fori_loop(0, C, body, 0)

    for q in range(C):
        g_ready(0, q)
    g_second(0)
    g_second(1)
    gate_tiles(0, 0, C)
    g_second(2)
    g_second(3)
    run(UP, 3, n)
    for q in range(C):
        g_ready(1, q)
    gate_tiles(1, 0, C)
    service(DOWN, 1)
    finish(UP)
    up_tiles(0)
    run(DOWN, 2, 3)
    up_tiles(1)
    for p in range(1, parts):
        service(DOWN + p, 1)
    run(DOWN, 3, n)
    for p in range(1, parts):
        service(DOWN + p, 2)

    for p in range(parts):
        for k in range(1, nx + 1):
            for h in range(H):
                pair_copy(0, p, far(k), 0, h).wait_send()
                if k < nx:
                    mix_copy(p, k, h, x).wait_send()

    def sum_first(p):
        for e in (1, 0):
            for k in range(1, nx + 1):
                for h in range(H):
                    left = act[e * rows + h * rt : e * rows + (h + 1) * rt, :]
                    partials(1, p, far(k), e, h, left, down_buf)
        for e in (1, 0):
            for k in range(1, nx + 1):
                xo = far(k)
                for h in range(H):
                    value = both(1, p, xo, e, h)
                    if h == 0 and k < nx:
                        send_buf[p, xo, e, 0] = value.astype(bf16)
                        x_one(p, k, e).start()
                    elif h == 1 and e == 1:
                        send_buf[p, xo, 1, 1] = value.astype(bf16)
                        z_one(p, k).start()
                    else:
                        keep[p, xo, e, h] = value

    def sum_second(p):
        for k in range(1, nx):
            z_in = z_one(p, k)
            z_in.wait_recv()
            send_buf[p, far(k), 0, 1] = (
                keep[p, far(k), 0, 1] + arrived(p, far(k), 0, 1)
            ).astype(bf16)
            x_two(p, k).start()
        value = keep[p, x, 1, 0]
        for k in range(1, nx):
            x_one_in(p, k, 1).wait_recv()
            value = value + arrived(p, far(k), 1, 0)
        send_buf[p, x, 1, 0] = value.astype(bf16)
        z_two(p).start()

    def sum_last(p):
        cols = slice(p * bw, (p + 1) * bw)
        total = keep[p, x, 0, 0]
        for k in range(1, nx):
            x_one_in(p, k, 0).wait_recv()
            total = total + arrived(p, far(k), 0, 0)
        z_two(p).wait_recv()
        total = total + arrived(p, x, 0, 0)
        out[chunk(0), cols] = (res_buf[0, t, chunk(0), cols].astype(f32) + total).astype(bf16)
        z_one(p, nx).wait_recv()
        total = keep[p, x, 0, 1] + arrived(p, x, 0, 1)
        for k in range(1, nx):
            x_two_in(p, k).wait_recv()
            total = total + arrived(p, far(k), 1, 1)
        out[chunk(1), cols] = (res_buf[0, t, chunk(1), cols].astype(f32) + total).astype(bf16)

    def sum_drain(p):
        for k in range(1, nx + 1):
            z_one(p, k).wait_send()
            for e in range(2):
                for h in range(H):
                    pair_copy(1, p, far(k), e, h).wait_send()
                if k < nx:
                    x_one(p, k, e).wait_send()
            if k < nx:
                x_two(p, k).wait_send()
        z_two(p).wait_send()

    finish(DOWN)
    sum_first(0)
    for p in range(1, parts):
        run(DOWN + p, 3, n)
        sum_second(p - 1)
        finish(DOWN + p)
        sum_first(p)
        sum_last(p - 1)
    sum_second(parts - 1)
    sum_last(parts - 1)

    for p in range(parts):
        sum_drain(p)
    for h in range(H):
        for k in range(nx):
            ag_x(k, h).wait_send()
        for k in range(1, nx):
            ag_fwd(k, h).wait_send()
    g_drain()
    for k in range(streams):
        drain(k)


def local(
    dims,
    tokens,
    mix_gain,
    w_u,
    w_v,
    u_scale,
    v_scale,
    spatial,
    spatial_bias,
    w_mix,
    mix_scale,
    ffn_gain,
    w_gate,
    w_up,
    gate_scale,
    up_scale,
    w_down,
    down_scale,
):
    n, n_tp = dims
    nx = n_tp // 2
    rows, dt = tokens.shape
    dr, ff = w_gate.shape
    df = mix_scale.shape[1]
    parts = 2 if df % 256 == 0 else 1
    streams = 4 + parts
    wide = up_to(-(-ff // 2), 128)
    rt, bw = rows // H, dt // parts
    hbm = pl.BlockSpec(memory_space=pl.ANY)
    vmem = pl.BlockSpec(memory_space=pltpu.VMEM)
    dma = pltpu.SemaphoreType.DMA
    sums = (parts, nx, 2, H, rt, bw)
    return pl.pallas_call(
        functools.partial(layer_kernel, (n, n_tp, parts)),
        out_shape=jax.ShapeDtypeStruct((rows, dt), bf16),
        in_specs=[hbm, vmem, vmem] + [hbm] * 6 + [vmem] * 8,
        out_specs=vmem,
        scratch_shapes=[
            pltpu.VMEM((2,) + w_u.shape, f32),
            pltpu.VMEM(w_mix.shape, f32),
            pltpu.VMEM(w_gate.shape, f32),
            pltpu.VMEM(w_up.shape, f32),
            pltpu.VMEM((n, dr, 2 * w_u.shape[1]), bf16),
            pltpu.VMEM((n,) + w_mix.shape, bf16),
            pltpu.VMEM((n + 1, dr, wide), bf16),
            pltpu.VMEM((n + 1, dr, wide), bf16),
            pltpu.VMEM((n + 1, wide, df), bf16),
            pltpu.VMEM((n_tp, rows, dt), bf16),
            pltpu.VMEM((2, n_tp, rows, dt), bf16),
            pltpu.VMEM((rows, w_u.shape[1]), bf16),
            pltpu.VMEM((2 * rows, wide), f32),
            pltpu.VMEM((2 * rows, wide), bf16),
            pltpu.VMEM(sums, bf16),
            pltpu.VMEM(sums, bf16),
            pltpu.VMEM(sums, f32),
            pltpu.VMEM(sums, bf16),
            pltpu.VMEM(sums, bf16),
            dma((7,)),
            dma((streams, n + 4)),
            dma((streams, n)),
            dma((streams, n)),
            dma((streams, n)),
            dma((nx, H)),
            dma((nx, H)),
            dma((n_tp, H)),
            dma((nx, C)),
            dma((C,)),
            dma((2, nx, C)),
            dma((nx, C)),
            dma((nx, C)),
            dma((2, n_tp, C)),
            dma((2, parts, nx, 2, H)),
            dma((2, parts, nx, 2, H)),
            dma((parts, nx, H)),
            dma((parts, nx, H)),
            dma((parts, nx, 2, H)),
            dma((parts, nx, 2, H)),
        ],
        compiler_params=pltpu.CompilerParams(
            collective_id=0, has_side_effects=True, vmem_limit_bytes=67000000
        ),
    )(
        tokens,
        mix_gain.reshape(1, -1),
        ffn_gain.reshape(1, -1),
        w_u,
        w_v,
        w_mix,
        w_gate,
        w_up,
        w_down,
        u_scale.reshape(1, -1),
        v_scale.reshape(1, -1),
        spatial,
        spatial_bias,
        mix_scale,
        gate_scale.reshape(1, -1),
        up_scale.reshape(1, -1),
        down_scale,
    )


def solution(mesh):
    placed = (
        P(("grp", "fs"), "tp"),
        P(),
        P("fs", "tp"),
        P("fs", "tp"),
        P("tp"),
        P("tp"),
        P("tp", None, None),
        P("tp", None),
        P("tp", "fs"),
        P(None, "fs"),
        P(),
        P("fs", "tp"),
        P("fs", "tp"),
        P("tp"),
        P("tp"),
        P("tp", "fs"),
        P(None, "fs"),
    )
    dims = (mesh.shape["fs"], mesh.shape["tp"])
    return jax.shard_map(
        functools.partial(local, dims),
        mesh=mesh,
        in_specs=placed,
        out_specs=P(("grp", "fs"), "tp"),
        check_vma=False,
    )
```

time: 243 us -> 197 us (0.81)
  Pallas kernels: 223 us -> 192 us
  other arithmetic: 12.8 us -> 0 us
    pallas_call x1, Pallas kernels: 223 us -> 192 us  [local(): pl.pallas_call(functools.partial(layer_kernel, (n, n_tp, parts)), out_sha...]
    convert_element_type x4 -> x0, other arithmetic: 5.84 us -> none  [the longest x1 1.99 us: local(): w_mix.astype(half)]
    another operation x5 -> x0, other arithmetic: 5.49 us -> none
    reshape x0 -> x2, local copies, waits for them, and re-layouts: none -> 2.58 us  [the longest x1 1.29 us: local(): gate_scale.reshape(1, -1)]
where the time goes in v1:
time: 197 us; the launch traced here: 196 us
  Pallas kernels  192 us (97%)
  local copies, waits for them, and re-layouts  4.65 us (2%)
    pallas_call x1, Pallas kernels, local(): pl.pallas_call(functools.partial(layer_kernel, (n, n_tp, parts)), out_sha...  192 us

profile of v1, /device:TPU:0, one launch (start us, length us, event | category | flops | bytes accessed | tf_op | source)
XLA Modules:
  0.0 196.3 jit_solution(13724679062051249007)
XLA Ops:
  0.0 1.3 reshape.22.gate_scale
  1.3 1.3 reshape.23.up_scale
  2.6 191.6 %shard_map.163 = bf16[768,512]{1,0:T(8,128)(2,1)} custom-call(bf16[768,512]{1,0:T(8,128)(2,1)} %tokens.1, f32[1,2048]{1,0:T(1,128)} %bitcast.4, f32[1,2048]{1,0:T(1,128)} %bitcast.5, f32[512,256]{1,0:T(8,128)} %w_u.1, f32[512,256]{1,0:T(8,128)} %w_v.1, f32[256,512]{1,0:T(8,128)} %w_mix.1, f32[512,1408]{1,0:T(8,128)} %w_gate.1, f32[512,1408]{1,0:T(8,128)} %w_up.1, ...), custom_call_target="tpu_custom_call" | custom-call | tf_op jit(solution)/shard_map/pallas_call | solution.py:742
  194.2 2.1 %copy.19 = bf16[768,512]{1,0:T(8,128)(2,1)} copy(bf16[768,512]{1,0:T(8,128)(2,1)} %shard_map.163) | data formatting | bytes 1572864

commit v2 on v1

--- a/solution.py
+++ b/solution.py
@@ -11,6 +11,9 @@
 eps = 1e-06
 H = 2
 C = 4
+DIAG = 0
+GSUB = 2
+USUB = 4
 half_root = 0.7071067811865476
 f32 = jnp.float32
 bf16 = jnp.bfloat16
@@ -48,7 +51,8 @@
     mix_stage,
     gate_stage,
     up_stage,
-    uv_buf,
+    u_buf,
+    v_buf,
     mix_buf,
     gate_buf,
     up_buf,
@@ -79,8 +83,6 @@
     g_recv,
     p_send,
     p_recv,
-    m_send,
-    m_recv,
     f_send,
     f_recv,
 ):
@@ -90,7 +92,9 @@
     g = lax.axis_index("grp")
     t = lax.axis_index("tp")
     x, c = t // 2, t % 2
-    m = i % 2
+    quad = i % 4
+    odd = i % 2
+    m = jnp.where(jnp.logical_or(quad == 0, quad == 3), 1, 0)
     rows, dt = tokens.shape
     dr, ff = w_gate.shape
     df = w_down.shape[1]
@@ -104,7 +108,7 @@
     heights = (wide, rest)
     partner = {"tp": x * 2 + 1 - c}
     across = {"grp": 1 - g}
-    beside = {"fs": i + 1 - 2 * m}
+    beside = {"fs": i + 1 - 2 * odd}
 
     def far(k):
         return lax.rem(x + k, nx)
@@ -144,10 +148,19 @@
         pl.semaphore_signal(barrier, 1, device_id=far_id(k), device_id_type=MESH)
     pl.semaphore_wait(barrier, (n - 1) + 2 + (nx - 1))
 
-    UV, MIX, GATE, UP, DOWN = range(5)
-    bufs = (uv_buf, mix_buf, gate_buf, up_buf) + (down_buf,) * parts
+    U, V, MIX, GATE, UP, DOWN = 0, 1, 2, 3, 3 + GSUB, 3 + GSUB + USUB
+    cuts = df // 128
+    bufs = (u_buf, v_buf, mix_buf) + (gate_buf,) * GSUB + (up_buf,) * USUB + (down_buf,) * cuts
+    gates, ups = range(GATE, UP), range(UP, DOWN)
+    downs = [range(DOWN + p * cuts // parts, DOWN + (p + 1) * cuts // parts) for p in range(parts)]
     streams = len(bufs)
     dc = df // parts
+    steps = {
+        (1, True): jnp.where(odd == 0, 3, 1),
+        (1, False): jnp.where(odd == 0, 1, 2),
+        (-1, True): jnp.where(odd == 1, 3, 1),
+        (-1, False): jnp.where(odd == 1, 1, 2),
+    }
 
     def view(k, slot, who, h):
         ref = bufs[k]
@@ -155,12 +168,14 @@
             count = ref.shape[1] // 2
             return ref.at[slot, pl.ds(pl.multiple_of(who * count, 16), count), :]
         if k < DOWN:
-            count = dr // 2
-            sl = pl.ds(pl.multiple_of(who * count, 16), count)
+            subs, sub = (GSUB, k - GATE) if k < UP else (USUB, k - UP)
+            count = dr // (2 * subs)
+            first = (who * subs + sub) * count
+            sl = pl.ds(pl.multiple_of(first, 16), count)
             return ref.at[slot, sl, pl.ds(0, widths[h])]
         count = heights[h] // 2
         sl = pl.ds(pl.multiple_of(who * count, 16), count)
-        return ref.at[slot, sl, pl.ds((k - DOWN) * dc, dc)]
+        return ref.at[slot, sl, pl.ds((k - DOWN) * 128, 128)]
 
     def z_copy(k, src, dst, step, h, sem):
         return remote(
@@ -175,102 +190,109 @@
         ref = view(k, j, who, h)
         return remote(ref, ref, y_send.at[k, j], y_recv.at[k, j], across)
 
-    def by_half(k, f):
-        if k < GATE:
-            f(0)
-            return
+    def stride(k, way, same=True):
+        return 1 if k < GATE else steps[way, same]
+
+    def inside(target):
+        return jnp.logical_and(target >= 0, target < n)
+
+    def both_halves(f):
         for h in range(2):
 
             @pl.when(m == h)
             def _():
                 f(h)
 
-    def own_each(k, act_on):
-        stride = 1 if k < GATE else 2
-
-        def each(h):
-            if k >= GATE:
-
-                @pl.when(i + 1 < n)
+    def own_each(k, h, act_on, only=None):
+        for way in (1, -1):
+            for same in (True, False):
+                if k < GATE and not same:
+                    continue
+                step = way * stride(k, way, same)
+                fits = inside(i + step)
+                if k >= GATE:
+                    fits = jnp.logical_and(fits, m == (h if same else 1 - h))
+                if only is not None:
+                    fits = jnp.logical_and(fits, only)
+                src = i if same else n
+                sem = n + (0 if way > 0 else 1) + (0 if same else 2)
+
+                @pl.when(fits)
                 def _():
-                    act_on(z_copy(k, n, i, 1, 1 - h, n + 2))
-
-                @pl.when(i > 0)
-                def _():
-                    act_on(z_copy(k, n, i, -1, 1 - h, n + 3))
-
-            @pl.when(i + stride < n)
-            def _():
-                act_on(z_copy(k, i, i, stride, h, n))
-
-            @pl.when(i - stride >= 0)
-            def _():
-                act_on(z_copy(k, i, i, -stride, h, n + 1))
-
-        by_half(k, each)
-
-    def own(k):
-        own_each(k, lambda copy: copy.start())
-
-    def service(k, s):
+                    act_on(z_copy(k, src, i, step, h, sem))
+
+    def own(k, h=0):
+        own_each(k, h, lambda copy: copy.start())
+
+    def service(k, s, h=None, side="any"):
         if s >= n:
             return
-        stride = 1 if k < GATE else 2
-
-        def each(h):
-            left, right = i - s, i + s
-
-            @pl.when(left >= 0)
+        if k >= GATE and h is None:
+            service(k, s, 0, side)
+            service(k, s, 1, side)
+            return
+        for way in (1, -1):
+            j = i - way * s
+            here = inside(j)
+            if h is not None:
+                here = jnp.logical_and(here, m == h)
+            if side != "any":
+                here = jnp.logical_and(here, odd == (1 if (way > 0) == (side == "in") else 0))
+            step = way * stride(k, way)
+
+            @pl.when(here)
             def _():
-                z_copy(k, left, left, stride, h, left).wait_recv()
-
-                @pl.when(i + stride < n)
+                z_copy(k, j, j, step, h, j).wait_recv()
+
+                @pl.when(inside(i + step))
                 def _():
-                    z_copy(k, left, left, stride, h, left).start()
-
-                y_copy(k, left, g, h).start()
-
-            @pl.when(right < n)
-            def _():
-                z_copy(k, right, right, -stride, h, right).wait_recv()
-
-                @pl.when(i - stride >= 0)
-                def _():
-                    z_copy(k, right, right, -stride, h, right).start()
-
-                y_copy(k, right, g, h).start()
-
-        by_half(k, each)
-
-    def run(k, begin, end):
+                    z_copy(k, j, j, step, h, j).start()
+
+                y_copy(k, j, g, h).start()
+
+    def run(k, begin, end, h=None):
         for s in range(begin, end):
-            service(k, s)
+            service(k, s, h)
 
     def finish(k):
         def each(h):
             for s in range(1, n):
                 y_copy(k, lax.rem(i + s, n), 1 - g, h).wait_recv()
 
-        by_half(k, each)
+        if k < GATE:
+            each(0)
+        else:
+            both_halves(each)
+
+    def own_down(p):
+        if p < parts:
+            for k in downs[p]:
+                own(k, 0)
+                own(k, 1)
+
+    def finish_all(ks):
+        for k in ks:
+            finish(k)
 
     def drain(k):
-        stride = 1 if k < GATE else 2
-        own_each(k, lambda copy: copy.wait_send())
+        for h in range(1 if k < GATE else 2):
+            own_each(k, h, lambda copy: copy.wait_send())
 
         def each(h):
             for s in range(1, n):
                 j = lax.rem(i + s, n)
                 y_copy(k, j, g, h).wait_send()
-
-                @pl.when(jnp.logical_and(j < i, i + stride < n))
-                def _():
-                    z_copy(k, j, j, stride, h, j).wait_send()
-
-                @pl.when(jnp.logical_and(j > i, i - stride >= 0))
-                def _():
-                    z_copy(k, j, j, -stride, h, j).wait_send()
-
-        by_half(k, each)
+                for way in (1, -1):
+                    step = way * stride(k, way)
+
+                    @pl.when(jnp.logical_and(way * (i - j) > 0, inside(i + step)))
+                    def _():
+                        z_copy(k, j, j, step, h, j).wait_send()
+
+        if k < GATE:
+            each(0)
+        else:
+            both_halves(each)
 
     def chunk(h):
         return pl.ds(h * rt, rt)
@@ -334,11 +356,11 @@
     def g_first(q):
         for k in range(1, nx):
             gd(0, k, q).wait_recv()
-            if q < C // 2:
+            if q < DIAG:
                 gfz(k, q).start()
             gd(0, k, q).start()
         gd(1, 0, q).wait_recv()
-        if q >= C // 2:
+        if q >= DIAG:
             for k in range(1, nx):
                 gfx(k, q).start()
         gd(1, 0, q).start()
@@ -360,7 +382,7 @@
                     gd(e, k, q).wait_send()
             for k in range(1, nx):
                 gx(k, q).wait_send()
-                if q < C // 2:
+                if q < DIAG:
                     gfz(k, q).wait_send()
                 else:
                     gfx(k, q).wait_send()
@@ -375,17 +397,19 @@
         return remote(
             give_buf.at[p, xo, e, h],
             pair_buf.at[p, xo, e, h],
-            p_send.at[r, p, xo, e, h],
-            p_recv.at[r, p, xo, e, h],
+            p_send.at[p, xo, e, h],
+            p_recv.at[p, xo, e, h],
             partner,
         )
 
     def partials(r, p, xo, e, h, left, buf):
-        give_buf[p, xo, e, h] = jnp.dot(
-            left, weight(buf, xo * 2 + 1 - c, p), preferred_element_type=f32
-        ).astype(bf16)
+        right = jnp.concatenate(
+            [weight(buf, xo * 2 + 1 - c, p), weight(buf, xo * 2 + c, p)], axis=1
+        )
+        value = jnp.dot(left, right, preferred_element_type=f32)
+        give_buf[p, xo, e, h] = value[:, :bw].astype(bf16)
         pair_copy(r, p, xo, e, h).start()
-        keep[p, xo, e, h] = jnp.dot(left, weight(buf, xo * 2 + c, p), preferred_element_type=f32)
+        keep[p, xo, e, h] = value[:, bw:]
 
     def both(r, p, xo, e, h):
         pair_copy(r, p, xo, e, h).wait_recv()
@@ -396,8 +420,8 @@
         return remote(
             send_buf.at[p, xo, 0, h],
             far_buf.at[p, slot, 0, h],
-            m_send.at[p, xo, h],
-            m_recv.at[p, slot, h],
+            f_send.at[p, xo, 0, h],
+            f_recv.at[p, slot, 0, h],
             far_id(k),
         )
 
@@ -410,23 +434,23 @@
             device,
         )
 
-    def x_one(p, k, e):
-        return far_copy(p, (far(k), e, 0), (x, e, 0), far_id(k))
-
-    def x_one_in(p, k, e):
-        return far_copy(p, (far(k), e, 0), (far(k), e, 0), far_id(k))
-
-    def z_one(p, k):
-        return far_copy(p, (far(k), 1, 1), (far(k), 0, 1), beside)
-
-    def z_two(p):
-        return far_copy(p, (x, 1, 0), (x, 0, 0), beside)
-
-    def x_two(p, k):
-        return far_copy(p, (far(k), 0, 1), (x, 1, 1), far_id(k))
-
-    def x_two_in(p, k):
-        return far_copy(p, (far(k), 0, 1), (far(k), 1, 1), far_id(k))
+    def x_one(p, k, e, h):
+        return far_copy(p, (far(k), e, h), (x, e, h), far_id(k))
+
+    def x_one_in(p, k, e, h):
+        return far_copy(p, (far(k), e, h), (far(k), e, h), far_id(k))
+
+    def z_one(p, k, h):
+        return far_copy(p, (far(k), 1, h), (far(k), 0, h), beside)
+
+    def z_two(p, h):
+        return far_copy(p, (x, 1, h), (x, 0, h), beside)
+
+    def x_two(p, k, h):
+        return far_copy(p, (far(k), 0, h), (x, 1, h), far_id(k))
+
+    def x_two_in(p, k, h):
+        return far_copy(p, (far(k), 0, h), (far(k), 1, h), far_id(k))
 
     def arrived(p, a, e, h):
         return far_buf[p, a, e, h].astype(f32)
@@ -447,15 +471,19 @@
             ag_x(k, h).start()
     loads[0].wait()
     loads[1].wait()
-    for s in range(dr // 128):
-        sl = slice(s * 128, (s + 1) * 128)
-        gain = column(mix_gain, s)
-        uv_buf[i, sl, :width] = (uv_stage[0, sl, :] * gain * u_scale[0:1, :]).astype(bf16)
-        uv_buf[i, sl, width:] = (uv_stage[1, sl, :] * gain * v_scale[0:1, :]).astype(bf16)
-    own(UV)
+    for w, scale, buf in ((0, u_scale, u_buf), (1, v_scale, v_buf)):
+        for s in range(dr // 128):
+            sl = slice(s * 128, (s + 1) * 128)
+            gain = column(mix_gain, s)
+            buf[i, sl, :] = (uv_stage[w, sl, :] * gain * scale[0:1, :]).astype(bf16)
+        own((U, V)[w])
     loads[2].wait()
     mix_buf[i] = (mix_stage[...] * mix_scale[0:1, :]).astype(bf16)
-    own(MIX)
+
+    def lane_row(scale, lo, hi):
+        if scale.shape[0] == 1:
+            return scale[0:1, lo:hi]
+        return jnp.concatenate([scale[r : r + 1, :] for r in range(lo // 128, hi // 128)], axis=1)
 
     def cast_in(stage, scale, buf):
         for s in range(dr // 128):
@@ -464,7 +492,7 @@
             for h, (lo, hi) in enumerate(((0, wide), (wide, ff))):
                 slot = jnp.where(m == h, i, n)
                 buf[slot, sl, : hi - lo] = (
-                    stage[sl, lo:hi] * gain * scale[0:1, lo:hi]
+                    stage[sl, lo:hi] * gain * lane_row(scale, lo, hi)
                 ).astype(bf16)
                 if hi - lo < widths[h]:
                     buf[slot, sl, hi - lo : widths[h]] = jnp.zeros(
@@ -489,10 +517,23 @@
             down_buf[j, rest:, :] = jnp.zeros((wide - rest, df), bf16)
 
     for s in range(1, n):
-        service(UV, s)
-        service(MIX, s)
+        service(U, s)
+        service(V, s)
         if s == max(n - 2, 1):
-            own(GATE)
+            own(MIX)
+    near = max(n - 1, 2)
+
+    def own_at(ks, half, who):
+        for k in ks:
+            own_each(k, half, lambda copy: copy.start(), m == who)
+
+    def service_all(ks, s, h=None, side="any"):
+        for k in ks:
+            service(k, s, h, side)
+
+    own_at(gates, 0, 1)
+    run(MIX, 1, near, 0)
+    own_at(gates, 0, 0)
     for h in range(H):
         for k in range(1, nx):
             ag_fwd(k, h).wait_recv()
@@ -501,7 +542,9 @@
         for k in range(nx):
             ag_in(k, h).wait_recv()
     loads[6].wait()
-    finish(UV)
+    finish(U)
+    service(MIX, 1, 1)
+    finish(V)
 
     groups, span = spatial.shape[0], spatial.shape[1]
     lanes = width // groups
@@ -515,10 +558,10 @@
 
     for h in range(H):
         left = gather_rows([tok_buf[q, chunk(h), :] for q in range(n_tp)])
-        pre = jnp.dot(left, uv_buf[...].reshape(-1, 2 * width), preferred_element_type=f32)
-        pre = pre * factor(left)
-        u = gelu(pre[:, :width])
-        v = gelu(pre[:, width:]).astype(bf16)
+        inv = factor(left)
+        u = gelu(jnp.dot(left, u_buf[...].reshape(-1, width), preferred_element_type=f32) * inv)
+        v = jnp.dot(left, v_buf[...].reshape(-1, width), preferred_element_type=f32) * inv
+        v = gelu(v).astype(bf16)
         for q in range(groups):
             mat = jnp.where(causal, spatial[q].astype(f32), 0.0).astype(bf16)
             cols = slice(q * lanes, (q + 1) * lanes)
@@ -528,6 +571,14 @@
                 gated[h * rt + b * span : h * rt + (b + 1) * span, cols] = (
                     u[sl, cols] * mixed
                 ).astype(bf16)
+        if h == 0:
+            run(MIX, 2, near, 1)
+    run(MIX, near, n)
+    for k in gates:
+        own(k, 1)
+    service_all(gates, 1, 0, "in")
+    for k in ups:
+        own(k, 0)
     finish(MIX)
 
     for k in range(1, nx):
@@ -538,12 +589,9 @@
             for p in range(parts):
                 send_buf[p, far(k), 0, h] = both(0, p, far(k), 0, h).astype(bf16)
                 mix_copy(p, k, h, x).start()
-    service(GATE, 1)
-    own(UP)
     for h in range(H):
         for p in range(parts):
             partials(0, p, x, 0, h, gated[chunk(h), :], mix_buf)
-    service(GATE, 2)
     for h in range(H):
         for p in range(parts):
             total = both(0, p, x, 0, h)
@@ -556,16 +604,24 @@
             ).astype(bf16)
         for q in range(h * (C // H), (h + 1) * (C // H)):
             g_start(q)
-    run(GATE, 3, n)
-    service(UP, 1)
+        if h == 0:
+            service(GATE, 1, 1)
+            service_all(gates, 1, 0, "out")
+    service_all(ups, 1, 0, "in")
+    for k in ups:
+        own(k, 1)
+    own_down(0)
     g_first(0)
+    service_all(gates[1:], 1, 1)
+    service(GATE, 2)
     g_first(1)
-    service(UP, 2)
-    for k in range(parts):
-        own(DOWN + k)
+    service_all(gates[1:], 2)
+    for k in gates:
+        run(k, 3, n)
     g_first(2)
+    service_all(ups, 1, 0, "out")
     g_first(3)
-    finish(GATE)
+    finish_all(gates)
 
     def gate_tiles(e, begin, end):
         def body(b, carry):
@@ -593,25 +649,38 @@
 
     for q in range(C):
         g_ready(0, q)
-    g_second(0)
-    g_second(1)
     gate_tiles(0, 0, C)
-    g_second(2)
-    g_second(3)
-    run(UP, 3, n)
     for q in range(C):
-        g_ready(1, q)
-    gate_tiles(1, 0, C)
-    service(DOWN, 1)
-    finish(UP)
+        g_second(q)
+        for k in ups[q : q + 1]:
+            service(k, 1, 1)
+            service(k, 2)
+            run(k, 3, n)
+        if q == 1:
+            service_all(downs[0], 1, 0, "in")
+            own_down(1)
+        if q == C - 2:
+            for e in range(C):
+                g_ready(1, e) if e < C - 2 else None
+            gate_tiles(1, 0, C - 2)
+    g_ready(1, C - 2)
+    g_ready(1, C - 1)
+    gate_tiles(1, C - 2, C)
+    for k in downs[0][:1]:
+        service(k, 1, 1)
+        service(k, 2, 1)
+        run(k, 3, n, 1)
+    finish_all(ups)
     up_tiles(0)
-    run(DOWN, 2, 3)
+    service_all(downs[0], 1, 0, "out")
+    for k in downs[0][1:]:
+        service(k, 1, 1)
+        service(k, 2, 1)
+        run(k, 3, n, 1)
     up_tiles(1)
-    for p in range(1, parts):
-        service(DOWN + p, 1)
-    run(DOWN, 3, n)
-    for p in range(1, parts):
-        service(DOWN + p, 2)
+    for k in downs[0]:
+        service(k, 2, 0)
+        run(k, 3, n, 0)
 
     for p in range(parts):
         for k in range(1, nx + 1):
@@ -620,79 +689,109 @@
                 if k < nx:
                     mix_copy(p, k, h, x).wait_send()
 
+    def z_first(p, h):
+        return h == 1
+
     def sum_first(p):
-        for e in (1, 0):
-            for k in range(1, nx + 1):
-                for h in range(H):
-                    left = act[e * rows + h * rt : e * rows + (h + 1) * rt, :]
-                    partials(1, p, far(k), e, h, left, down_buf)
-        for e in (1, 0):
-            for k in range(1, nx + 1):
-                xo = far(k)
-                for h in range(H):
-                    value = both(1, p, xo, e, h)
-                    if h == 0 and k < nx:
-                        send_buf[p, xo, e, 0] = value.astype(bf16)
-                        x_one(p, k, e).start()
-                    elif h == 1 and e == 1:
-                        send_buf[p, xo, 1, 1] = value.astype(bf16)
-                        z_one(p, k).start()
-                    else:
-                        keep[p, xo, e, h] = value
+        order = [(e, k, h) for e in (1, 0) for k in range(1, nx + 1) for h in range(H)]
+
+        def pass_on(e, k, h):
+            xo = far(k)
+            value = both(1, p, xo, e, h)
+            if not z_first(p, h) and k < nx:
+                send_buf[p, xo, e, h] = value.astype(bf16)
+                x_one(p, k, e, h).start()
+            elif z_first(p, h) and e == 1:
+                send_buf[p, xo, 1, h] = value.astype(bf16)
+                z_one(p, k, h).start()
+            else:
+                keep[p, xo, e, h] = value
+
+        lag = 4
+        for a, (e, k, h) in enumerate(order):
+            left = act[e * rows + h * rt : e * rows + (h + 1) * rt, :]
+            partials(1, p, far(k), e, h, left, down_buf)
+            if a >= lag:
+                pass_on(*order[a - lag])
+        for a in range(len(order) - lag, len(order)):
+            pass_on(*order[a])
 
     def sum_second(p):
-        for k in range(1, nx):
-            z_in = z_one(p, k)
-            z_in.wait_recv()
-            send_buf[p, far(k), 0, 1] = (
-                keep[p, far(k), 0, 1] + arrived(p, far(k), 0, 1)
-            ).astype(bf16)
-            x_two(p, k).start()
-        value = keep[p, x, 1, 0]
-        for k in range(1, nx):
-            x_one_in(p, k, 1).wait_recv()
-            value = value + arrived(p, far(k), 1, 0)
-        send_buf[p, x, 1, 0] = value.astype(bf16)
-        z_two(p).start()
+        for h in range(H):
+            if z_first(p, h):
+                for k in range(1, nx):
+                    z_one(p, k, h).wait_recv()
+                    send_buf[p, far(k), 0, h] = (
+                        keep[p, far(k), 0, h] + arrived(p, far(k), 0, h)
+                    ).astype(bf16)
+                    x_two(p, k, h).start()
+            else:
+                value = keep[p, x, 1, h]
+                for k in range(1, nx):
+                    x_one_in(p, k, 1, h).wait_recv()
+                    value = value + arrived(p, far(k), 1, h)
+                send_buf[p, x, 1, h] = value.astype(bf16)
+                z_two(p, h).start()
 
     def sum_last(p):
         cols = slice(p * bw, (p + 1) * bw)
-        total = keep[p, x, 0, 0]
-        for k in range(1, nx):
-            x_one_in(p, k, 0).wait_recv()
-            total = total + arrived(p, far(k), 0, 0)
-        z_two(p).wait_recv()
-        total = total + arrived(p, x, 0, 0)
-        out[chunk(0), cols] = (res_buf[0, t, chunk(0), cols].astype(f32) + total).astype(bf16)
-        z_one(p, nx).wait_recv()
-        total = keep[p, x, 0, 1] + arrived(p, x, 0, 1)
-        for k in range(1, nx):
-            x_two_in(p, k).wait_recv()
-            total = total + arrived(p, far(k), 1, 1)
-        out[chunk(1), cols] = (res_buf[0, t, chunk(1), cols].astype(f32) + total).astype(bf16)
+        for h in range(H):
+            total = keep[p, x, 0, h]
+            if z_first(p, h):
+                z_one(p, nx, h).wait_recv()
+                total = total + arrived(p, x, 0, h)
+                for k in range(1, nx):
+                    x_two_in(p, k, h).wait_recv()
+                    total = total + arrived(p, far(k), 1, h)
+            else:
+                for k in range(1, nx):
+                    x_one_in(p, k, 0, h).wait_recv()
+                    total = total + arrived(p, far(k), 0, h)
+                z_two(p, h).wait_recv()
+                total = total + arrived(p, x, 0, h)
+            out[chunk(h), cols] = (
+                res_buf[0, t, chunk(h), cols].astype(f32) + total
+            ).astype(bf16)
 
     def sum_drain(p):
-        for k in range(1, nx + 1):
-            z_one(p, k).wait_send()
-            for e in range(2):
-                for h in range(H):
+        for h in range(H):
+            for k in range(1, nx + 1):
+                for e in range(2):
                     pair_copy(1, p, far(k), e, h).wait_send()
-                if k < nx:
-                    x_one(p, k, e).wait_send()
-            if k < nx:
-                x_two(p, k).wait_send()
-        z_two(p).wait_send()
-
-    finish(DOWN)
+                if z_first(p, h):
+                    z_one(p, k, h).wait_send()
+                    if k < nx:
+                        x_two(p, k, h).wait_send()
+                elif k < nx:
+                    for e in range(2):
+                        x_one(p, k, e, h).wait_send()
+            if not z_first(p, h):
+                z_two(p, h).wait_send()
+
+    for p in range(1, parts):
+        service_all(downs[p], 1, 0, "in")
+    finish_all(downs[0])
+    for p in range(1, parts):
+        for k in downs[p][:1]:
+            service(k, 1, 1)
+            service(k, 2, 1)
+            run(k, 3, n, 1)
     sum_first(0)
     for p in range(1, parts):
-        run(DOWN + p, 3, n)
-        sum_second(p - 1)
-        finish(DOWN + p)
+        for k in downs[p][1:]:
+            service(k, 1, 1)
+            service(k, 2, 1)
+            run(k, 3, n, 1)
+        service_all(downs[p], 1, 0, "out")
+        for k in downs[p]:
+            service(k, 2, 0)
+            run(k, 3, n, 0)
+        finish_all(downs[p])
         sum_first(p)
-        sum_last(p - 1)
-    sum_second(parts - 1)
-    sum_last(parts - 1)
+    for p in range(parts):
+        sum_second(p)
+    for p in range(parts):
+        sum_last(p)
 
     for p in range(parts):
         sum_drain(p)
@@ -704,6 +803,10 @@
     g_drain()
     for k in range(streams):
         drain(k)
+
+
+def lane_rows(scale):
+    return scale.reshape(-1, 128) if scale.shape[0] % 128 == 0 else scale.reshape(1, -1)
 
 
 def local(
@@ -732,7 +835,7 @@
     dr, ff = w_gate.shape
     df = mix_scale.shape[1]
     parts = 2 if df % 256 == 0 else 1
-    streams = 4 + parts
+    streams = 3 + GSUB + USUB + df // 128
     wide = up_to(-(-ff // 2), 128)
     rt, bw = rows // H, dt // parts
     hbm = pl.BlockSpec(memory_space=pl.ANY)
@@ -749,7 +852,8 @@
             pltpu.VMEM(w_mix.shape, f32),
             pltpu.VMEM(w_gate.shape, f32),
             pltpu.VMEM(w_up.shape, f32),
-            pltpu.VMEM((n, dr, 2 * w_u.shape[1]), bf16),
+            pltpu.VMEM((n,) + w_u.shape, bf16),
+            pltpu.VMEM((n,) + w_v.shape, bf16),
             pltpu.VMEM((n,) + w_mix.shape, bf16),
             pltpu.VMEM((n + 1, dr, wide), bf16),
             pltpu.VMEM((n + 1, dr, wide), bf16),
@@ -778,10 +882,8 @@
             dma((nx, C)),
             dma((nx, C)),
             dma((2, n_tp, C)),
-            dma((2, parts, nx, 2, H)),
-            dma((2, parts, nx, 2, H)),
-            dma((parts, nx, H)),
-            dma((parts, nx, H)),
+            dma((parts, nx, 2, H)),
+            dma((parts, nx, 2, H)),
             dma((parts, nx, 2, H)),
             dma((parts, nx, 2, H)),
         ],
@@ -803,8 +905,8 @@
         spatial,
         spatial_bias,
         mix_scale,
-        gate_scale.reshape(1, -1),
-        up_scale.reshape(1, -1),
+        lane_rows(gate_scale),
+        lane_rows(up_scale),
         down_scale,
     )
 

time: 197 us -> 161 us (0.82)
  Pallas kernels: 192 us -> 159 us
  local copies, waits for them, and re-layouts: 4.65 us -> 2.06 us
    pallas_call x1, Pallas kernels: 192 us -> 159 us  [local(): pl.pallas_call(functools.partial(layer_kernel, (n, n_tp, parts)), out_sha...]
    reshape x2 -> x0, local copies, waits for them, and re-layouts: 2.58 us -> none  [the longest x1 1.29 us: local(): gate_scale.reshape(1, -1)]
where the time goes in v2:
time: 161 us
  Pallas kernels  159 us (99%)
  local copies, waits for them, and re-layouts  2.06 us (1%)
    pallas_call x1, Pallas kernels, local(): pl.pallas_call(functools.partial(layer_kernel, (n, n_tp, parts)), out_sha...  159 us

profile of v2, /device:TPU:0, one launch (start us, length us, event | category | flops | bytes accessed | tf_op | source)
XLA Modules:
  0.0 160.6 jit_solution(2339489518086847481)
XLA Ops:
  0.0 158.6 %shard_map.163 = bf16[768,512]{1,0:T(8,128)(2,1)} custom-call(bf16[768,512]{1,0:T(8,128)(2,1)} %tokens.1, f32[1,2048]{1,0:T(1,128)} %bitcast.6, f32[1,2048]{1,0:T(1,128)} %bitcast.7, f32[512,256]{1,0:T(8,128)} %w_u.1, f32[512,256]{1,0:T(8,128)} %w_v.1, f32[256,512]{1,0:T(8,128)} %w_mix.1, f32[512,1408]{1,0:T(8,128)} %w_gate.1, f32[512,1408]{1,0:T(8,128)} %w_up.1, ...), custom_call_target="tpu_custom_call" | custom-call | tf_op jit(solution)/shard_map/pallas_call | solution.py:845
  158.6 2.1 %copy.19 = bf16[768,512]{1,0:T(8,128)(2,1)} copy(bf16[768,512]{1,0:T(8,128)(2,1)} %shard_map.163) | data formatting | bytes 1572864

commit v3 on v2

--- a/solution.py
+++ b/solution.py
@@ -148,9 +148,12 @@
         pl.semaphore_signal(barrier, 1, device_id=far_id(k), device_id_type=MESH)
     pl.semaphore_wait(barrier, (n - 1) + 2 + (nx - 1))
 
-    U, V, MIX, GATE, UP, DOWN = 0, 1, 2, 3, 3 + GSUB, 3 + GSUB + USUB
+    U, V, MIX = 0, 1, 2
+    GATE = MIX + parts
+    UP = GATE + GSUB
+    DOWN = UP + USUB
     cuts = df // 128
-    bufs = (u_buf, v_buf, mix_buf) + (gate_buf,) * GSUB + (up_buf,) * USUB + (down_buf,) * cuts
+    bufs = (u_buf, v_buf) + (mix_buf,) * parts + (gate_buf,) * GSUB + (up_buf,) * USUB + (down_buf,) * cuts
     gates, ups = range(GATE, UP), range(UP, DOWN)
     downs = [range(DOWN + p * cuts // parts, DOWN + (p + 1) * cuts // parts) for p in range(parts)]
     streams = len(bufs)
@@ -166,7 +169,9 @@
         ref = bufs[k]
         if k < GATE:
             count = ref.shape[1] // 2
-            return ref.at[slot, pl.ds(pl.multiple_of(who * count, 16), count), :]
+            first, cols = (0, width) if k < MIX else ((k - MIX) * dc, dc)
+            sl = pl.ds(pl.multiple_of(who * count, 16), count)
+            return ref.at[slot, sl, pl.ds(first, cols)]
         if k < DOWN:
             subs, sub = (GSUB, k - GATE) if k < UP else (USUB, k - UP)
             count = dr // (2 * subs)
@@ -203,7 +208,7 @@
             def _():
                 f(h)
 
-    def own_each(k, h, act_on, only=None):
+    def own_each(k, h, act_on, only=None, side=None):
         for way in (1, -1):
             for same in (True, False):
                 if k < GATE and not same:
@@ -214,15 +219,18 @@
                     fits = jnp.logical_and(fits, m == (h if same else 1 - h))
                 if only is not None:
                     fits = jnp.logical_and(fits, only)
+                if side is not None:
+                    to_pair = jnp.logical_and(odd == (0 if way > 0 else 1), not same)
+                    fits = jnp.logical_and(fits, to_pair == (side == "in"))
                 src = i if same else n
-                sem = n + (0 if way > 0 else 1) + (0 if same else 2)
+                sem = {(1, True): i, (-1, True): n, (1, False): n + 1, (-1, False): n + 2}[way, same]
 
                 @pl.when(fits)
                 def _():
                     act_on(z_copy(k, src, i, step, h, sem))
 
-    def own(k, h=0):
-        own_each(k, h, lambda copy: copy.start())
+    def own(k, h=0, side=None):
+        own_each(k, h, lambda copy: copy.start(), None, side)
 
     def service(k, s, h=None, side="any"):
         if s >= n:
@@ -264,11 +272,11 @@
         else:
             both_halves(each)
 
-    def own_down(p):
+    def own_down(p, side=None):
         if p < parts:
             for k in downs[p]:
                 own(k, 0)
-                own(k, 1)
+                own(k, 1, side)
 
     def finish_all(ks):
         for k in ks:
@@ -520,8 +528,10 @@
         service(U, s)
         service(V, s)
         if s == max(n - 2, 1):
-            own(MIX)
+            for k in range(MIX, GATE):
+                own(k)
     near = max(n - 1, 2)
+    mixes = range(MIX, GATE)
 
     def own_at(ks, half, who):
         for k in ks:
@@ -531,8 +541,18 @@
         for k in ks:
             service(k, s, h, side)
 
+    def far_in(ks):
+        if n <= 4:
+            for k in ks:
+                run(k, 2, n, 1)
+
+    def near_in(ks):
+        for k in ks:
+            run(k, 1, 2 if n <= 4 else n, 1)
+
     own_at(gates, 0, 1)
-    run(MIX, 1, near, 0)
+    for s in range(1, near):
+        service_all(mixes, s, 0)
     own_at(gates, 0, 0)
     for h in range(H):
         for k in range(1, nx):
@@ -543,7 +563,7 @@
             ag_in(k, h).wait_recv()
     loads[6].wait()
     finish(U)
-    service(MIX, 1, 1)
+    service_all(mixes, 1, 1)
     finish(V)
 
     groups, span = spatial.shape[0], spatial.shape[1]
@@ -572,26 +592,26 @@
                     u[sl, cols] * mixed
                 ).astype(bf16)
         if h == 0:
-            run(MIX, 2, near, 1)
-    run(MIX, near, n)
+            for s in range(2, near):
+                service_all(mixes, s, 1)
+    for s in range(near, n):
+        service_all(mixes, s)
     for k in gates:
         own(k, 1)
     service_all(gates, 1, 0, "in")
     for k in ups:
         own(k, 0)
-    finish(MIX)
-
-    for k in range(1, nx):
-        for h in range(H):
-            for p in range(parts):
+    for p in range(parts):
+        finish(MIX + p)
+        for k in range(1, nx):
+            for h in range(H):
                 partials(0, p, far(k), 0, h, gated[chunk(h), :], mix_buf)
         for h in range(H):
-            for p in range(parts):
+            partials(0, p, x, 0, h, gated[chunk(h), :], mix_buf)
+        for k in range(1, nx):
+            for h in range(H):
                 send_buf[p, far(k), 0, h] = both(0, p, far(k), 0, h).astype(bf16)
                 mix_copy(p, k, h, x).start()
-    for h in range(H):
-        for p in range(parts):
-            partials(0, p, x, 0, h, gated[chunk(h), :], mix_buf)
     for h in range(H):
         for p in range(parts):
             total = both(0, p, x, 0, h)
@@ -605,22 +625,27 @@
         for q in range(h * (C // H), (h + 1) * (C // H)):
             g_start(q)
         if h == 0:
-            service(GATE, 1, 1)
             service_all(gates, 1, 0, "out")
+            far_in(gates)
     service_all(ups, 1, 0, "in")
     for k in ups:
-        own(k, 1)
-    own_down(0)
-    g_first(0)
-    service_all(gates[1:], 1, 1)
-    service(GATE, 2)
-    g_first(1)
-    service_all(gates[1:], 2)
+        own(k, 1, "in")
+    own(DOWN, 0)
+    near_in(gates)
+    service(GATE, 2, 0)
+    service_all(gates[1:], 2, 0)
     for k in gates:
-        run(k, 3, n)
-    g_first(2)
+        run(k, 3, n, 0)
+    for q in range(C - 1):
+        g_first(q)
     service_all(ups, 1, 0, "out")
-    g_first(3)
+    g_first(C - 1)
+    for k in ups:
+        own(k, 1, "out")
+    for k in downs[0][1:]:
+        own(k, 0)
+    if n <= 4:
+        service(UP, 1, 1)
     finish_all(gates)
 
     def gate_tiles(e, begin, end):
@@ -636,7 +661,7 @@
 
         lax.fori_loop(begin, end, body, 0)
 
-    def up_tiles(e):
+    def up_tiles(e, begin, end):
         def body(b, carry):
             sl = pl.ds(pl.multiple_of(b * ct, 64), ct)
             flat = pl.ds(pl.multiple_of(e * rows + b * ct, 64), ct)
@@ -645,42 +670,44 @@
             act[flat, :] = (silu_buf[flat, :] * a).astype(bf16)
             return carry
 
-        lax.fori_loop(0, C, body, 0)
+        lax.fori_loop(begin, end, body, 0)
 
     for q in range(C):
         g_ready(0, q)
-    gate_tiles(0, 0, C)
+    gate_tiles(0, 0, C // 2)
+    run(UP, 2, n, 0)
+    far_in(ups[:1])
+    gate_tiles(0, C // 2, C)
     for q in range(C):
         g_second(q)
-        for k in ups[q : q + 1]:
-            service(k, 1, 1)
-            service(k, 2)
-            run(k, 3, n)
+        for k in ups[max(q, 1) : q + 1]:
+            run(k, 2, n, 0)
+            far_in([k])
         if q == 1:
             service_all(downs[0], 1, 0, "in")
+            for k in downs[0]:
+                own(k, 1)
             own_down(1)
         if q == C - 2:
             for e in range(C):
                 g_ready(1, e) if e < C - 2 else None
             gate_tiles(1, 0, C - 2)
+    near_in(ups[1:] if n <= 4 else ups)
     g_ready(1, C - 2)
     g_ready(1, C - 1)
     gate_tiles(1, C - 2, C)
-    for k in downs[0][:1]:
-        service(k, 1, 1)
-        service(k, 2, 1)
-        run(k, 3, n, 1)
+    far_in(downs[0][:1])
+    near_in(downs[0][:1])
     finish_all(ups)
-    up_tiles(0)
+    up_tiles(0, 0, C // 2)
+    far_in(downs[0][1:])
+    near_in(downs[0][1:])
+    up_tiles(0, C // 2, C)
     service_all(downs[0], 1, 0, "out")
-    for k in downs[0][1:]:
-        service(k, 1, 1)
-        service(k, 2, 1)
-        run(k, 3, n, 1)
-    up_tiles(1)
+    up_tiles(1, 0, C // 2)
     for k in downs[0]:
-        service(k, 2, 0)
-        run(k, 3, n, 0)
+        run(k, 2, n, 0)
+    up_tiles(1, C // 2, C)
 
     for p in range(parts):
         for k in range(1, nx + 1):
@@ -692,7 +719,7 @@
     def z_first(p, h):
         return h == 1
 
-    def sum_first(p):
+    def sum_first(p, hook):
         order = [(e, k, h) for e in (1, 0) for k in range(1, nx + 1) for h in range(H)]
 
         def pass_on(e, k, h):
@@ -713,6 +740,8 @@
             partials(1, p, far(k), e, h, left, down_buf)
             if a >= lag:
                 pass_on(*order[a - lag])
+            if a == lag:
+                hook()
         for a in range(len(order) - lag, len(order)):
             pass_on(*order[a])
 
@@ -771,27 +800,24 @@
     for p in range(1, parts):
         service_all(downs[p], 1, 0, "in")
     finish_all(downs[0])
+
+    def later(k):
+        far_in([k])
+        near_in([k])
+        service(k, 1, 0, "out")
+        run(k, 2, n, 0)
+
+    rest_downs = [k for p in range(1, parts) for k in downs[p]]
+    for k in rest_downs[:1]:
+        later(k)
+    sum_first(0, lambda: [later(k) for k in rest_downs[1:]])
     for p in range(1, parts):
-        for k in downs[p][:1]:
-            service(k, 1, 1)
-            service(k, 2, 1)
-            run(k, 3, n, 1)
-    sum_first(0)
-    for p in range(1, parts):
-        for k in downs[p][1:]:
-            service(k, 1, 1)
-            service(k, 2, 1)
-            run(k, 3, n, 1)
-        service_all(downs[p], 1, 0, "out")
-        for k in downs[p]:
-            service(k, 2, 0)
-            run(k, 3, n, 0)
         finish_all(downs[p])
-        sum_first(p)
-    for p in range(parts):
-        sum_second(p)
-    for p in range(parts):
-        sum_last(p)
+        sum_second(p - 1)
+        sum_first(p, lambda: None)
+        sum_last(p - 1)
+    sum_second(parts - 1)
+    sum_last(parts - 1)
 
     for p in range(parts):
         sum_drain(p)
@@ -835,7 +861,7 @@
     dr, ff = w_gate.shape
     df = mix_scale.shape[1]
     parts = 2 if df % 256 == 0 else 1
-    streams = 3 + GSUB + USUB + df // 128
+    streams = 2 + parts + GSUB + USUB + df // 128
     wide = up_to(-(-ff // 2), 128)
     rt, bw = rows // H, dt // parts
     hbm = pl.BlockSpec(memory_space=pl.ANY)
@@ -869,7 +895,7 @@
             pltpu.VMEM(sums, bf16),
             pltpu.VMEM(sums, bf16),
             dma((7,)),
-            dma((streams, n + 4)),
+            dma((streams, n + 3)),
             dma((streams, n)),
             dma((streams, n)),
             dma((streams, n)),
@@ -879,7 +905,7 @@
             dma((nx, C)),
             dma((C,)),
             dma((2, nx, C)),
-            dma((nx, C)),
+            dma((nx, max(DIAG, 1))),
             dma((nx, C)),
             dma((2, n_tp, C)),
             dma((parts, nx, 2, H)),

time: 161 us -> 156 us (0.969)
  Pallas kernels: 159 us -> 154 us
    pallas_call x1, Pallas kernels: 159 us -> 154 us  [local(): pl.pallas_call(functools.partial(layer_kernel, (n, n_tp, parts)), out_sha...]
where the time goes in v3:
time: 156 us
  Pallas kernels  154 us (99%)
  local copies, waits for them, and re-layouts  2.06 us (1%)
    pallas_call x1, Pallas kernels, local(): pl.pallas_call(functools.partial(layer_kernel, (n, n_tp, parts)), out_sha...  154 us

profile of v3, /device:TPU:0, one launch (start us, length us, event | category | flops | bytes accessed | tf_op | source)
XLA Modules:
  0.0 155.7 jit_solution(3498356092534799)
XLA Ops:
  0.0 153.6 %shard_map.163 = bf16[768,512]{1,0:T(8,128)(2,1)} custom-call(bf16[768,512]{1,0:T(8,128)(2,1)} %tokens.1, f32[1,2048]{1,0:T(1,128)} %bitcast.6, f32[1,2048]{1,0:T(1,128)} %bitcast.7, f32[512,256]{1,0:T(8,128)} %w_u.1, f32[512,256]{1,0:T(8,128)} %w_v.1, f32[256,512]{1,0:T(8,128)} %w_mix.1, f32[512,1408]{1,0:T(8,128)} %w_gate.1, f32[512,1408]{1,0:T(8,128)} %w_up.1, ...), custom_call_target="tpu_custom_call" | custom-call | tf_op jit(solution)/shard_map/pallas_call | solution.py:871
  153.6 2.1 %copy.19 = bf16[768,512]{1,0:T(8,128)(2,1)} copy(bf16[768,512]{1,0:T(8,128)(2,1)} %shard_map.163) | data formatting | bytes 1572864
